TPU v7x, 512 devices: a whole 4x8x8 slice. The times are simulated.
512 devices in a mesh: sp: 32 (over z, x), tp: 16 (over y, core).
Axes of the slice: x: 4, y: 8, z: 8, core: 2. Of those that a mesh axis runs over, the one named last changes fastest.
Arguments:
- latent: bfloat16 [16384, 2048], P('sp'), may hold values from -6 to 6
- context: bfloat16 [512, 2048], P('sp'), may hold values from -6 to 6
- condition: bfloat16 [2048], replicated, may hold values from -6 to 6
- context_condition: bfloat16 [2048], replicated, may hold values from -6 to 6
- shift_weight: bfloat16 [2048, 2048], P('sp', 'tp'), may hold values from -0.125 to 0.125
- scale_weight: bfloat16 [2048, 2048], P('sp', 'tp'), may hold values from -0.125 to 0.125
- mod_gate_weight: bfloat16 [2048, 2048], P('sp', 'tp'), may hold values from -0.5 to 0.5
- norm_gain: bfloat16 [2048], replicated, may hold values from 0.099609375 to 1.8984375
- query_weight: bfloat16 [2048, 2048], P(None, 'tp'), may hold values from -0.125 to 0.125
- key_weight: bfloat16 [2048, 2048], P(None, 'tp'), may hold values from -0.125 to 0.125
- value_weight: bfloat16 [2048, 2048], P(None, 'tp'), may hold values from -0.125 to 0.125
- gate_weight: bfloat16 [2048, 2048], P(None, 'tp'), may hold values from -0.125 to 0.125
- forward_decay: float32 [16], P('tp'), may hold values from 0 to 1, as said below
- backward_decay: float32 [16], P('tp'), may hold values from 0 to 1, as said below
- out_weight: bfloat16 [2048, 2048], P('tp'), may hold values from -0.125 to 0.125
Outputs:
- mixed: bfloat16 [16384, 2048], P('sp')
Inputs may be any that keep to these rules, and one draw needn't show every extreme that they name: `forward_decay`: each head's rate is positive. `backward_decay`: each head's rate is positive.
All inputs are finite; a program needn't handle non-finite values.
Results may differ from a plain program's by a relative error of at most 0.015.
Values may be sent and summed in bfloat16 or wider, within the bound.
No kernel may reach another device: no remote copies, remote signals or barrier semaphores. Data moves between devices by JAX's collectives and lax.ppermute only.
A program may use at most 64 MiB of HBM per device.

v0:
```python
import jax
import jax.numpy as jnp
from jax import lax
from jax.sharding import Mesh
from jax.sharding import PartitionSpec as P

HEAD_DIM = 128
GRID_W = 64
SP = ("sp_0", "sp_1")
EPS = 1e-06
THETA = 10000.0
CONTEXT_LIFT = 3.0
TOP_PRECISION = lax.Precision.HIGHEST


def sent_to_all(x, axis):
    copies = jnp.broadcast_to(x, (lax.axis_size(axis), *x.shape))
    return lax.all_to_all(copies, axis, split_axis=0, concat_axis=0, tiled=True)


def taken_together(x, axis):
    everything = sent_to_all(x, axis)
    return jnp.sum(everything, axis=0)


def in_one(arrays, axis):
    ravelled, at, finished = (jnp.concatenate([a.reshape(-1) for a in arrays]), 0, [])
    total = lax.psum(ravelled, axis)
    for a in arrays:
        finished.append(total[at : at + a.size].reshape(a.shape))
        at += a.size
    return tuple(finished)


def filled_with(x, identity):
    return jax.tree.map(
        lambda a, e: jnp.broadcast_to(jnp.asarray(e, a.dtype), a.shape), x, identity
    )


def all_in_one(x, axis):
    leaves = jax.tree.leaves(x)
    order = sorted(range(len(leaves)), key=lambda k: -leaves[k].size)
    width = (1, *leaves[order[0]].shape)[-1]
    lines = [
        jnp.pad(leaves[k].reshape(-1), (0, -leaves[k].size % width)).reshape(-1, width)
        for k in order
    ]
    both, at, found = (lax.all_gather(jnp.concatenate(lines), axis), 0, {})
    for k, line in zip(order, lines):
        slab = both[:, at : at + len(line)].reshape(len(both), -1)
        found[k] = slab[:, : leaves[k].size].reshape(-1, *leaves[k].shape)
        at += len(line)
    numbers = iter(range(len(leaves)))
    return jax.tree.map(lambda _: found[next(numbers)], x)


def prefix_by_axis(x, axes, combine, identity, reverse):
    before = start = filled_with(x, identity)
    total = x
    for axis in reversed(axes):
        length, mine = (lax.axis_size(axis), lax.axis_index(axis))
        pieces = all_in_one(total, axis)
        inside, total = (start, start)
        for k in reversed(range(length)) if reverse else range(length):
            passed = k > mine if reverse else k < mine
            total = combine(total, jax.tree.map(lambda part: part[k], pieces))
            inside = jax.tree.map(lambda new, old: jnp.where(passed, new, old), total, inside)
        before = combine(inside, before)
    return before


def laid_out(parts, dim):
    dims = list(parts.shape[1:])
    dims[dim] *= parts.shape[0]
    return jnp.moveaxis(parts, 0, dim).reshape(dims)


def collect(x, axis, dim):
    return laid_out(sent_to_all(x, axis), dim)


def modulated(token_rows, norm_gain, shifts, scales):
    values = token_rows.astype(jnp.float32)
    values = values * lax.rsqrt(jnp.mean(values * values, axis=-1, keepdims=True) + EPS)
    values = values * norm_gain.astype(jnp.float32)
    return (values * (1.0 + scales) + shifts).astype(jnp.bfloat16)


def rope_half(portion, positions):
    quarter = portion.shape[-1] // 2
    frequency = THETA ** (-jnp.arange(quarter, dtype=jnp.float32) / quarter)
    angles = positions[:, None, None] * frequency
    cosine = jnp.cos(angles)
    sine_table = jnp.sin(angles)
    leading = portion[..., :quarter]
    trailing = portion[..., quarter:]
    return jnp.concatenate(
        [leading * cosine - trailing * sine_table, leading * sine_table + trailing * cosine],
        axis=-1,
    )


def rotate(values, grid_row, grid_column):
    half_width = values.shape[-1] // 2
    return jnp.concatenate(
        [
            rope_half(values[..., :half_width], grid_row),
            rope_half(values[..., half_width:], grid_column),
        ],
        axis=-1,
    )


def combine(earlier, later):
    return (earlier[0] * later[0], later[0][:, None, None] * earlier[1] + later[1])


def local(
    latent,
    context,
    condition,
    context_condition,
    shift_weight,
    scale_weight,
    mod_gate_weight,
    norm_gain,
    query_weight,
    key_weight,
    value_weight,
    gate_weight,
    forward_decay,
    backward_decay,
    out_weight,
):
    sp_index = lax.axis_index(SP)
    tp_index = lax.axis_index("tp")
    sp_count = lax.axis_size(SP)
    tp_count = lax.axis_size("tp")
    tokens_here = latent.shape[0]
    local_rows = tokens_here // tp_count
    mod_rows = shift_weight.shape[0]
    activation = jax.nn.silu(jnp.stack([condition, context_condition]).astype(jnp.float32)).astype(
        jnp.bfloat16
    )
    own_part = lax.dynamic_slice_in_dim(activation, sp_index * mod_rows, mod_rows, 1)
    partial_value = jnp.stack(
        [
            jnp.dot(own_part, matrix, preferred_element_type=jnp.float32)
            for matrix in (shift_weight, scale_weight, mod_gate_weight)
        ]
    )
    summed = taken_together(partial_value, SP)
    modulation = lax.all_gather(summed, "tp", axis=2, tiled=True)
    hidden = modulated(latent, norm_gain, modulation[0, 0], modulation[1, 0])
    context_hidden = modulated(context, norm_gain, modulation[0, 1], modulation[1, 1])
    local_width = query_weight.shape[1]
    head_count = local_width // HEAD_DIM
    stacked = jnp.concatenate([query_weight, key_weight, value_weight, gate_weight], axis=1)
    projected = jnp.dot(hidden, stacked, preferred_element_type=jnp.float32).astype(jnp.bfloat16)
    queries = projected[:, :local_width]
    keys_out = projected[:, local_width : 2 * local_width]
    values_out = projected[:, 2 * local_width : 3 * local_width]
    out_gates = projected[:, 3 * local_width :]
    context_pairs = jnp.dot(
        context_hidden,
        stacked[:, local_width : 3 * local_width],
        preferred_element_type=jnp.float32,
    ).astype(jnp.bfloat16)

    def to_heads(values):
        return values.astype(jnp.float32).reshape(values.shape[0], head_count, HEAD_DIM)

    positions = sp_index * tokens_here + jnp.arange(tokens_here, dtype=jnp.int32)
    grid_row = (positions // GRID_W).astype(jnp.float32)
    grid_column = (positions % GRID_W).astype(jnp.float32)
    key_scale = HEAD_DIM ** (-0.5)
    query_heads = jnp.transpose(rotate(to_heads(queries), grid_row, grid_column), (1, 0, 2))
    key_heads = (
        jnp.transpose(rotate(to_heads(keys_out), grid_row, grid_column), (1, 0, 2)) * key_scale
    )
    value_heads = jnp.transpose(to_heads(values_out), (1, 0, 2))
    log_forward = -forward_decay
    log_backward = -backward_decay
    context_rows = context.shape[0]
    context_total = context_rows * sp_count
    context_index = (sp_index * context_rows + jnp.arange(context_rows, dtype=jnp.int32)).astype(
        jnp.float32
    )
    weight_forward = jnp.exp(log_forward[:, None] * (context_total - 1.0 - context_index)[None, :])
    weight_backward = jnp.exp(log_backward[:, None] * context_index[None, :])
    context_key_heads = to_heads(context_pairs[:, :local_width]) * (key_scale * CONTEXT_LIFT)
    context_value_heads = to_heads(context_pairs[:, local_width:])
    context_forward = jnp.einsum(
        "hc,chd,che->hde",
        weight_forward,
        context_key_heads,
        context_value_heads,
        precision=TOP_PRECISION,
    )
    context_backward = jnp.einsum(
        "hc,chd,che->hde",
        weight_backward,
        context_key_heads,
        context_value_heads,
        precision=TOP_PRECISION,
    )
    context_forward, context_backward = in_one((context_forward, context_backward), SP)
    offsets = jnp.arange(tokens_here, dtype=jnp.float32)
    distance = offsets[:, None] - offsets[None, :]
    mixing = jnp.where(
        distance >= 0, jnp.exp(log_forward[:, None, None] * jnp.maximum(distance, 0.0)), 0.0
    )
    mixing = mixing + jnp.where(
        distance <= 0, jnp.exp(log_backward[:, None, None] * jnp.maximum(-distance, 0.0)), 0.0
    )
    score_matrix = (
        jnp.einsum("htd,hsd->hts", query_heads, key_heads, precision=TOP_PRECISION) * mixing
    )
    local_out = jnp.einsum("hts,hse->hte", score_matrix, value_heads, precision=TOP_PRECISION)
    tail_forward = jnp.exp(log_forward[:, None] * (tokens_here - 1.0 - offsets)[None, :])
    head_backward = jnp.exp(log_backward[:, None] * offsets[None, :])
    own_forward = jnp.einsum(
        "ht,htd,hte->hde", tail_forward, key_heads, value_heads, precision=TOP_PRECISION
    )
    own_backward = jnp.einsum(
        "ht,htd,hte->hde", head_backward, key_heads, value_heads, precision=TOP_PRECISION
    )
    span_forward = jnp.exp(log_forward * tokens_here)
    span_backward = jnp.exp(log_backward * tokens_here)
    identity = (jnp.ones_like(span_forward), jnp.zeros_like(own_forward))
    before = prefix_by_axis((span_forward, own_forward), SP, combine, identity, False)
    after = prefix_by_axis((span_backward, own_backward), SP, combine, identity, True)
    device_start = (sp_index * tokens_here).astype(jnp.float32)
    device_rest = ((sp_count - 1 - sp_index) * tokens_here).astype(jnp.float32)
    incoming_forward = (
        before[1] + jnp.exp(log_forward * device_start)[:, None, None] * context_forward
    )
    incoming_backward = (
        after[1] + jnp.exp(log_backward * device_rest)[:, None, None] * context_backward
    )
    read_forward = jnp.exp(log_forward[:, None] * (offsets + 1.0)[None, :])[
        :, :, None
    ] * jnp.einsum("htd,hde->hte", query_heads, incoming_forward, precision=TOP_PRECISION)
    read_backward = jnp.exp(log_backward[:, None] * (tokens_here - offsets)[None, :])[
        :, :, None
    ] * jnp.einsum("htd,hde->hte", query_heads, incoming_backward, precision=TOP_PRECISION)
    retained = local_out + read_forward + read_backward
    retained = retained * lax.rsqrt(jnp.mean(retained * retained, axis=-1, keepdims=True) + EPS)
    merged = jnp.transpose(retained, (1, 0, 2)).reshape(tokens_here, local_width)
    heads_out = (jax.nn.silu(out_gates.astype(jnp.float32)) * merged).astype(jnp.bfloat16)
    projection = lax.psum_scatter(
        jnp.dot(heads_out, out_weight, preferred_element_type=jnp.float32),
        "tp",
        scatter_dimension=0,
        tiled=True,
    )
    own_latent = lax.dynamic_slice_in_dim(latent, tp_index * local_rows, local_rows, 0)
    finished = (own_latent.astype(jnp.float32) + modulation[2, 0] * projection).astype(jnp.bfloat16)
    return collect(finished, "tp", 0)


def solution(mesh):
    torus = Mesh(mesh.devices.reshape(8, 4, mesh.shape["tp"]), ("sp_0", "sp_1", "tp"))
    in_specs = (
        P(SP, None),
        P(SP, None),
        P(),
        P(),
        P(SP, "tp"),
        P(SP, "tp"),
        P(SP, "tp"),
        P(),
        P(None, "tp"),
        P(None, "tp"),
        P(None, "tp"),
        P(None, "tp"),
        P("tp"),
        P("tp"),
        P("tp", None),
    )
    out_specs = P(SP, None)
    return jax.shard_map(local, mesh=torus, in_specs=in_specs, out_specs=out_specs, check_vma=False)
```

profile of v0, /device:TPU:1, one launch (start us, length us, event | category | flops | bytes accessed | tf_op | source)
XLA Modules:
  0.0 352.9 jit_solution(17837896909596042663)
XLA Ops:
  6.5 0.8 stack.21
  7.4 0.7 stack.22
  8.1 0.9 convolution_bitcast_fusion.4
  9.0 0.9 convolution_bitcast_fusion.3
  9.9 0.9 convolution_bitcast_fusion.2
  10.9 0.7 broadcast_in_dim.10
  11.5 13.7 %all-to-all-start = ((f32[32,3,2,128]{3,2,1,0:T(2,128)}), f32[32,3,2,128]{3,2,1,0:T(2,128)S(1)}, u32[]{:S(2)}, u32[]{:S(2)}) async-start(f32[32,3,2,128]{3,2,1,0:T(2,128)} %broadcast_in_dim.10), calls=%async_computation | async-start | bytes 196608 | tf_op jit(solution)/shard_map/all_to_all | solution.py:18
  25.3 0.0 all-reduce.6.cloned.1.call-start
  27.0 1.0 fusion.45
  28.0 2.1 fusion
  30.0 0.7 convert_element_type.83
  30.7 3.6 %all-to-all-done = f32[32,3,2,128]{3,2,1,0:T(2,128)S(1)} async-done(((f32[32,3,2,128]{3,2,1,0:T(2,128)}), f32[32,3,2,128]{3,2,1,0:T(2,128)S(1)}, u32[]{:S(2)}, u32[]{:S(2)}) %all-to-all-start) | async-done | bytes 98336 | tf_op jit(solution)/shard_map/all_to_all | solution.py:18
  34.4 0.1 reduce_sum.36
  34.4 19.6 %all_gather.27 = f32[3,2,2048]{2,1,0:T(2,128)S(1)} all-gather(f32[3,2,128]{2,1,0:T(2,128)S(1)} %reduce_sum.36), channel_id=1, replica_groups=mesh['sp_0'=8,'sp_1'=4,'tp'=16] {'tp'}, dimensions={2}, use_global_device_ids=true | all-gather | bytes 52224 | tf_op jit(solution)/shard_map/all_gather | solution.py:154
  54.1 1.5 convolution_convert_fusion
  55.6 0.3 convolution_bitcast_fusion.1
  55.9 0.3 convolution_bitcast_fusion
  56.2 0.7 pad_maximum_fusion
  56.9 0.0 all-reduce.6.cloned.1.call-update
  56.9 0.0 reduce-scatter.2.cloned.1.call-start
  57.0 2.9 fusion.18
  59.9 0.1 fusion.53
  60.0 0.6 fusion.82
  60.6 0.3 fusion.40
  60.8 0.3 fusion.42
  61.1 9.4 %all-gather.4 = f32[4,129,128]{2,1,0:T(8,128)S(1)} all-gather(f32[1,129,128]{2,1,0:T(8,128)S(1)} %maximum_bitcast_fusion.4), channel_id=2, replica_groups=mesh['sp_0'=8,'sp_1'=4,'tp'=16] {'sp_1'}, dimensions={0}, use_global_device_ids=true | all-gather | bytes 330240 | tf_op jit(solution)/shard_map/all_gather | solution.py:49
  70.6 0.6 fusion.227
  74.4 9.7 %all-gather.6 = f32[4,129,128]{2,1,0:T(8,128)S(1)} all-gather(f32[1,129,128]{2,1,0:T(8,128)S(1)} %maximum_bitcast_fusion.6), channel_id=4, replica_groups=mesh['sp_0'=8,'sp_1'=4,'tp'=16] {'sp_1'}, dimensions={0}, use_global_device_ids=true | all-gather | bytes 330240 | tf_op jit(solution)/shard_map/all_gather | solution.py:49
  84.1 0.6 fusion.226
  89.2 2.0 fusion.233
  91.1 19.6 %all-gather.7 = f32[8,129,128]{2,1,0:T(8,128)S(1)} all-gather(f32[1,129,128]{2,1,0:T(8,128)S(1)} %maximum_bitcast_fusion.7), channel_id=5, replica_groups=mesh['sp_0'=8,'sp_1'=4,'tp'=16] {'sp_0'}, dimensions={0}, use_global_device_ids=true | all-gather | bytes 594432 | tf_op jit(solution)/shard_map/all_gather | solution.py:49
  110.7 0.7 fusion.224
  111.4 1.9 fusion.234
  113.3 20.3 %all-gather.5 = f32[8,129,128]{2,1,0:T(8,128)S(1)} all-gather(f32[1,129,128]{2,1,0:T(8,128)S(1)} %maximum_bitcast_fusion.5), channel_id=3, replica_groups=mesh['sp_0'=8,'sp_1'=4,'tp'=16] {'sp_0'}, dimensions={0}, use_global_device_ids=true | all-gather | bytes 594432 | tf_op jit(solution)/shard_map/all_gather | solution.py:49
  133.7 0.7 fusion.225
  135.6 1.5 convolution_multiply_fusion
  137.2 0.7 fusion.62
  137.9 61.9 %all-reduce.6.cloned.1.call-done = f32[32768]{0:T(1024)} async-done(((f32[32768]{0:T(1024)}), f32[32768]{0:T(1024)}) %all-reduce.6.cloned.1.call-update) | async-done | bytes 131088 | tf_op jit(solution)/shard_map/psum | solution.py:28
  199.9 8.0 %fusion.24 = f32[512,128]{0,1:T(8,128)S(1)} fusion(f32[512,128]{0,1:T(8,128)S(1)} %fusion.62, f32[512]{0:T(512)S(1)} %multiply_exponential_fusion.1, f32[32768]{0:T(1024)} %all-reduce.6.cloned.1.call-done, f32[8,129,128]{2,1,0:T(8,128)} %copy-done.3, f32[4,129,128]{2,1,0:T(8,128)S(1)} %all-gather.4, f32[512,1,32]{0,2,1:T(8,128)} %copy-done.5, ...), kind=kOutput, calls=%fused_computation.26 | convolution fusion | flops 101695488 | bytes 1847816 | tf_op jit(solution)/shard_map/htd,hde->hte/dot_general | solution.py:244
  207.9 8.0 %multiply_reduce_fusion = (f32[512]{0:T(512)S(1)}, f32[512,128]{0,1:T(8,128)S(1)}) fusion(f32[512,128]{0,1:T(8,128)S(1)} %fusion.24, f32[32768]{0:T(1024)} %all-reduce.6.cloned.1.call-done, f32[8,129,128]{2,1,0:T(8,128)} %copy-done.2, f32[4,129,128]{2,1,0:T(8,128)S(1)} %all-gather.6, f32[]{:T(128)} %bitcast.75, f32[]{:T(128)} %bitcast.76, f32[]{:T(128)} %bitcast.77, ...), kind=kOutput, calls=%fused_computation.53 | convolution fusion | flops 101826048 | bytes 1849864 | tf_op jit(solution)/shard_map/htd,hde->hte/dot_general | solution.py:247
  215.9 0.0 copy-done
  215.9 3.6 %fusion.50 = f32[512,2048]{1,0:T(8,128)} fusion(bf16[128,2048]{1,0:T(8,128)(2,1)S(1)} %copy-done, f32[512,128]{0,1:T(8,128)S(1)} %get-tuple-element.53, bf16[512,512]{0,1:T(8,128)(2,1)} %copy-done.4, f32[512]{0:T(512)S(1)} %add_rsqrt_fusion), kind=kOutput, calls=%fused_computation.66 | convolution fusion | flops 268959744 | bytes 5113856 | tf_op jit(solution)/shard_map/dot_general | solution.py:253
  219.5 0.0 reduce-scatter.2.cloned.1.call-update
  219.5 66.3 %reduce-scatter.2.cloned.1.call-done = f32[32,2048]{1,0:T(8,128)} async-done(((f32[512,2048]{1,0:T(8,128)}), f32[32,2048]{1,0:T(8,128)}) %reduce-scatter.2.cloned.1.call-update) | async-done | bytes 262160 | tf_op jit(solution)/shard_map/reduce_scatter | solution.py:252
  285.8 1.0 add_convert_fusion
  286.8 0.2 broadcast_in_dim.12
  287.1 57.7 %all_to_all.10 = bf16[16,32,2048]{2,1,0:T(8,128)(2,1)S(1)} all-to-all(bf16[16,32,2048]{2,1,0:T(8,128)(2,1)S(1)} %broadcast_in_dim.12), channel_id=1, replica_groups=mesh['sp_0'=8,'sp_1'=4,'tp'=16] {'tp'}, dimensions={0} | all-to-all | bytes 4194304 | tf_op jit(solution)/shard_map/all_to_all | solution.py:18
  344.8 1.3 copy.34
  (42 shorter events, 0.3 us)
Async XLA Ops:
  6.5 209.4 %copy-start = (bf16[128,2048]{1,0:T(8,128)(2,1)S(1)}, bf16[128,2048]{1,0:T(8,128)(2,1)}, u32[]{:S(2)}) copy-start(bf16[128,2048]{1,0:T(8,128)(2,1)} %param.29) | copy-start | bytes 1572868
  6.5 50.4 %copy-start.1 = (bf16[512,2048]{1,0:T(8,128)(2,1)S(1)}, bf16[512,2048]{1,0:T(8,128)(2,1)}, u32[]{:S(2)}) copy-start(bf16[512,2048]{1,0:T(8,128)(2,1)} %param.15) | copy-start | bytes 6291460
  6.5 50.4 %copy-start.8 = (bf16[2048,128]{1,0:T(8,128)(2,1)S(1)}, bf16[2048,128]{1,0:T(8,128)(2,1)}, u32[]{:S(2)}) copy-start(bf16[2048,128]{1,0:T(8,128)(2,1)} %param.25) | copy-start | bytes 1572868
  11.5 22.8 %all-to-all-start = ((f32[32,3,2,128]{3,2,1,0:T(2,128)}), f32[32,3,2,128]{3,2,1,0:T(2,128)S(1)}, u32[]{:S(2)}, u32[]{:S(2)}) async-start(f32[32,3,2,128]{3,2,1,0:T(2,128)} %broadcast_in_dim.10), calls=%async_computation | async-start | bytes 196608 | tf_op jit(solution)/shard_map/all_to_all | solution.py:18
  25.3 174.6 %all-reduce.6.cloned.1.call-start = ((), (), s32[]{:S(2)}) async-start(), calls=%async_computation.3 | async-start | bytes 262144 | tf_op jit(solution)/shard_map/psum | solution.py:28
  56.9 228.9 %reduce-scatter.2.cloned.1.call-start = ((), (), s32[]{:S(2)}) async-start(), calls=%async_computation.4 | async-start | bytes 4456448 | tf_op jit(solution)/shard_map/reduce_scatter | solution.py:252
  59.9 77.3 %copy-start.4 = (bf16[512,512]{0,1:T(8,128)(2,1)}, bf16[512,512]{0,1:T(8,128)(2,1)S(1)}, u32[]{:S(2)}) copy-start(bf16[512,512]{0,1:T(8,128)(2,1)S(1)} %fusion.18) | copy-start | bytes 1572868
  60.5 76.6 %copy-start.5 = (f32[512,1,32]{0,2,1:T(8,128)}, f32[512,1,32]{0,2,1:T(8,128)S(1)}, u32[]{:S(2)}) copy-start(f32[512,1,32]{0,2,1:T(8,128)S(1)} %get-tuple-element.25) | copy-start | bytes 196612
  60.5 76.6 %copy-start.6 = (f32[512,1,32]{0,2,1:T(8,128)}, f32[512,1,32]{0,2,1:T(8,128)S(1)}, u32[]{:S(2)}) copy-start(f32[512,1,32]{0,2,1:T(8,128)S(1)} %get-tuple-element.26) | copy-start | bytes 196612
  60.6 76.6 %copy-start.7 = (f32[512,1,32]{0,2,1:T(8,128)}, f32[512,1,32]{0,2,1:T(8,128)S(1)}, u32[]{:S(2)}) copy-start(f32[512,1,32]{0,2,1:T(8,128)S(1)} %get-tuple-element.27) | copy-start | bytes 196612
  110.7 24.9 %copy-start.2 = (f32[8,129,128]{2,1,0:T(8,128)}, f32[8,129,128]{2,1,0:T(8,128)S(1)}, u32[]{:S(2)}) copy-start(f32[8,129,128]{2,1,0:T(8,128)S(1)} %all-gather.7) | copy-start | bytes 1585156
  133.7 2.0 copy-start.3
Sparse Core Ops, SparseCore 0:
  57.0 142.7 all-reduce.5
  219.6 66.1 reduce-scatter.1
where the time goes:
time: 354 us; the launch traced here: 353 us
  blocking collectives  136 us (38%)
  waiting for transfers between devices  132 us (37%)
  matrix products  30.2 us (9%)
  between operations  24.2 us (7%)
  starting transfers between devices  13.8 us (4%)
  other arithmetic  10.1 us (3%)
  local copies, waits for them, and re-layouts  6.43 us (2%)
    reduce_scatter x1, waiting for transfers between devices, local(): lax.psum_scatter(jnp.dot(heads_out, out_weight, preferred_element_type=jn...  66.3 us
    psum x1, waiting for transfers between devices, in_one(): total = lax.psum(ravelled, axis)  61.9 us
    all_gather x4, blocking collectives, all_in_one(): both, at, found = (lax.all_gather(jnp.concatenate(lines), axis), 0, {})  59 us
    all_to_all x1, blocking collectives, sent_to_all(): return lax.all_to_all(copies, axis, split_axis=0, concat_axis=0, tiled=True)  57.7 us
    all_gather x1, blocking collectives, local(): modulation = lax.all_gather(summed, 'tp', axis=2, tiled=True)  19.6 us
    all_to_all x1, starting transfers between devices, sent_to_all(): return lax.all_to_all(copies, axis, split_axis=0, concat_axis=0, tiled=True)  13.7 us
    dot_general x1, matrix products, local(): jnp.einsum('htd,hde->hte', query_heads, incoming_forward, precision=TOP_P...  8.03 us
    dot_general x1, matrix products, local(): jnp.einsum('htd,hde->hte', query_heads, incoming_backward, precision=TOP_...  7.98 us
  transfers between devices with their start and end apart: 3, of which 3 were waited for; matrix products, arithmetic and copies ran while one was open for 5% of the time, Pallas kernels for 0%

commit v1 on v0

--- a/solution.py
+++ b/solution.py
@@ -151,7 +151,21 @@
         ]
     )
     summed = taken_together(partial_value, SP)
-    modulation = lax.all_gather(summed, "tp", axis=2, tiled=True)
+    ways, here, hop = (lax.axis_size("tp"), lax.axis_index("tp"), summed.shape[2])
+    shape = [n * ways if d == 2 else n for d, n in enumerate(summed.shape)]
+    full = lax.dynamic_update_slice_in_dim(
+        jnp.zeros(shape, summed.dtype), summed, here * hop, axis=2
+    )
+    going_up = going_down = summed
+    for far in range(1, ways // 2 + 1):
+        going_up = lax.ppermute(going_up, "tp", [(d, (d + 1) % ways) for d in range(ways)])
+        full = lax.dynamic_update_slice_in_dim(full, going_up, (here - far) % ways * hop, axis=2)
+        if 2 * far < ways:
+            going_down = lax.ppermute(going_down, "tp", [(d, (d - 1) % ways) for d in range(ways)])
+            full = lax.dynamic_update_slice_in_dim(
+                full, going_down, (here + far) % ways * hop, axis=2
+            )
+    modulation = full
     hidden = modulated(latent, norm_gain, modulation[0, 0], modulation[1, 0])
     context_hidden = modulated(context, norm_gain, modulation[0, 1], modulation[1, 1])
     local_width = query_weight.shape[1]

time: 354 us -> 373 us (1.054)
  starting transfers between devices: 13.8 us -> 36.2 us
  blocking collectives: 136 us -> 117 us
  waiting for transfers between devices: 132 us -> 148 us
    ppermute x0 -> x15, starting transfers between devices: none -> 22.4 us  [the longest x7 13.5 us: local(): lax.ppermute(going_down, 'tp', [(d, (d - 1) % ways) for d in range(ways)])]
    all_gather x1 -> x0, blocking collectives: 19.6 us -> none  [local(): modulation = lax.all_gather(summed, 'tp', axis=2, tiled=True)]
    ppermute x0 -> x15, waiting for transfers between devices: none -> 9.76 us  [the longest x8 8.34 us: local(): lax.ppermute(going_up, 'tp', [(d, (d + 1) % ways) for d in range(ways)])]
    psum x1, waiting for transfers between devices: 61.9 us -> 68 us  [in_one(): total = lax.psum(ravelled, axis)]
  transfers between devices with their start and end apart: 3 -> 18, of which waited for: 3 -> 17; matrix products, arithmetic and copies ran while one was open for 5% -> 5% of each run, Pallas kernels for 0% -> 0%
where the time goes in v1:
time: 373 us; the launch traced here: 372 us
  waiting for transfers between devices  148 us (40%)
  blocking collectives  117 us (31%)
  starting transfers between devices  36.2 us (10%)
  matrix products  30 us (8%)
  between operations  24.2 us (6%)
  other arithmetic  10.1 us (3%)
  local copies, waits for them, and re-layouts  6.61 us (2%)
    psum x1, waiting for transfers between devices, in_one(): total = lax.psum(ravelled, axis)  68 us
    reduce_scatter x1, waiting for transfers between devices, local(): lax.psum_scatter(jnp.dot(heads_out, out_weight, preferred_element_type=jn...  66.3 us
    all_gather x4, blocking collectives, all_in_one(): both, at, found = (lax.all_gather(jnp.concatenate(lines), axis), 0, {})  59.7 us
    all_to_all x1, blocking collectives, sent_to_all(): return lax.all_to_all(copies, axis, split_axis=0, concat_axis=0, tiled=True)  57.4 us
    all_to_all x1, starting transfers between devices, sent_to_all(): return lax.all_to_all(copies, axis, split_axis=0, concat_axis=0, tiled=True)  13.7 us
    ppermute x7, starting transfers between devices, local(): lax.ppermute(going_down, 'tp', [(d, (d - 1) % ways) for d in range(ways)])  13.5 us
    ppermute x8, starting transfers between devices, local(): lax.ppermute(going_up, 'tp', [(d, (d + 1) % ways) for d in range(ways)])  8.94 us
    ppermute x8, waiting for transfers between devices, local(): lax.ppermute(going_up, 'tp', [(d, (d + 1) % ways) for d in range(ways)])  8.34 us
  transfers between devices with their start and end apart: 18, of which 17 were waited for; matrix products, arithmetic and copies ran while one was open for 5% of the time, Pallas kernels for 0%

profile of v1, /device:TPU:1, one launch (start us, length us, event | category | flops | bytes accessed | tf_op | source)
XLA Modules:
  0.0 371.8 jit_solution(7758503060309841547)
XLA Ops:
  6.5 0.8 stack.21
  7.4 0.7 stack.22
  8.1 0.9 convolution_bitcast_fusion.4
  9.0 0.9 convolution_bitcast_fusion.3
  9.9 0.9 convolution_bitcast_fusion.2
  10.9 0.7 broadcast_in_dim.13
  11.5 13.7 %all-to-all-start = ((f32[32,3,2,128]{3,2,1,0:T(2,128)}), f32[32,3,2,128]{3,2,1,0:T(2,128)S(1)}, u32[]{:S(2)}, u32[]{:S(2)}) async-start(f32[32,3,2,128]{3,2,1,0:T(2,128)} %broadcast_in_dim.13), calls=%async_computation | async-start | bytes 196608 | tf_op jit(solution)/shard_map/all_to_all | solution.py:18
  27.2 1.0 fusion.45
  28.2 2.1 fusion
  30.3 0.7 convert_element_type.83
  31.0 3.4 all-to-all-done
  34.4 3.3 collective-permute-start
  37.7 0.7 collective-permute-done
  38.4 2.3 collective-permute-start.2
  40.8 0.7 collective-permute-done.2
  41.5 2.3 collective-permute-start.4
  44.0 1.0 collective-permute-start.5
  45.0 0.6 collective-permute-done.4
  45.6 1.1 collective-permute-start.6
  47.1 2.2 collective-permute-start.7
  49.3 0.6 collective-permute-done.6
  50.1 3.4 collective-permute-start.9
  53.5 0.6 collective-permute-done.8
  54.3 3.4 collective-permute-start.11
  58.5 3.4 collective-permute-start.13
  62.8 4.0 %collective-permute-done.14 = f32[3,2,128]{2,1,0:T(2,128)S(1)} collective-permute-done((f32[3,2,128]{2,1,0:T(2,128)S(1)}, f32[3,2,128]{2,1,0:T(2,128)S(1)}, u32[]{:S(2)}, u32[]{:S(2)}) %collective-permute-start.14) | collective-permute-done | bytes 3104 | tf_op jit(solution)/shard_map/ppermute | solution.py:161
  66.8 1.5 convolution_convert_fusion
  69.0 0.7 pad_maximum_fusion
  69.8 2.9 fusion.18
  73.9 9.4 %all-gather.4 = f32[4,129,128]{2,1,0:T(8,128)S(1)} all-gather(f32[1,129,128]{2,1,0:T(8,128)S(1)} %maximum_bitcast_fusion.4), channel_id=2, replica_groups=mesh['sp_0'=8,'sp_1'=4,'tp'=16] {'sp_1'}, dimensions={0}, use_global_device_ids=true | all-gather | bytes 330240 | tf_op jit(solution)/shard_map/all_gather | solution.py:49
  83.3 0.6 fusion.227
  87.2 9.8 %all-gather.6 = f32[4,129,128]{2,1,0:T(8,128)S(1)} all-gather(f32[1,129,128]{2,1,0:T(8,128)S(1)} %maximum_bitcast_fusion.6), channel_id=4, replica_groups=mesh['sp_0'=8,'sp_1'=4,'tp'=16] {'sp_1'}, dimensions={0}, use_global_device_ids=true | all-gather | bytes 330240 | tf_op jit(solution)/shard_map/all_gather | solution.py:49
  101.8 1.8 fusion.233
  103.6 19.9 %all-gather.7 = f32[8,129,128]{2,1,0:T(8,128)S(1)} all-gather(f32[1,129,128]{2,1,0:T(8,128)S(1)} %maximum_bitcast_fusion.7), channel_id=5, replica_groups=mesh['sp_0'=8,'sp_1'=4,'tp'=16] {'sp_0'}, dimensions={0}, use_global_device_ids=true | all-gather | bytes 594432 | tf_op jit(solution)/shard_map/all_gather | solution.py:49
  123.5 0.7 fusion.224
  124.2 2.0 fusion.234
  126.2 20.6 %all-gather.5 = f32[8,129,128]{2,1,0:T(8,128)S(1)} all-gather(f32[1,129,128]{2,1,0:T(8,128)S(1)} %maximum_bitcast_fusion.5), channel_id=3, replica_groups=mesh['sp_0'=8,'sp_1'=4,'tp'=16] {'sp_0'}, dimensions={0}, use_global_device_ids=true | all-gather | bytes 594432 | tf_op jit(solution)/shard_map/all_gather | solution.py:49
  146.8 0.7 fusion.225
  148.8 1.5 convolution_multiply_fusion
  150.4 0.7 fusion.62
  151.1 68.0 %all-reduce.6.cloned.1.call-done = f32[32768]{0:T(1024)} async-done(((f32[32768]{0:T(1024)}), f32[32768]{0:T(1024)}) %all-reduce.6.cloned.1.call-update) | async-done | bytes 131088 | tf_op jit(solution)/shard_map/psum | solution.py:28
  219.1 7.9 %fusion.24 = f32[512,128]{0,1:T(8,128)S(1)} fusion(f32[512,128]{0,1:T(8,128)S(1)} %fusion.62, f32[512]{0:T(512)S(1)} %multiply_exponential_fusion.1, f32[32768]{0:T(1024)} %all-reduce.6.cloned.1.call-done, f32[8,129,128]{2,1,0:T(8,128)} %copy-done.3, f32[4,129,128]{2,1,0:T(8,128)S(1)} %all-gather.4, f32[512,1,32]{0,2,1:T(8,128)} %copy-done.5, ...), kind=kOutput, calls=%fused_computation.26 | convolution fusion | flops 101695488 | bytes 1847816 | tf_op jit(solution)/shard_map/htd,hde->hte/dot_general | solution.py:258
  227.1 7.9 %multiply_reduce_fusion = (f32[512]{0:T(512)S(1)}, f32[512,128]{0,1:T(8,128)S(1)}) fusion(f32[512,128]{0,1:T(8,128)S(1)} %fusion.24, f32[32768]{0:T(1024)} %all-reduce.6.cloned.1.call-done, f32[8,129,128]{2,1,0:T(8,128)} %copy-done.2, f32[4,129,128]{2,1,0:T(8,128)S(1)} %all-gather.6, f32[]{:T(128)} %bitcast.75, f32[]{:T(128)} %bitcast.76, f32[]{:T(128)} %bitcast.77, ...), kind=kOutput, calls=%fused_computation.53 | convolution fusion | flops 101826048 | bytes 1849864 | tf_op jit(solution)/shard_map/htd,hde->hte/dot_general | solution.py:261
  235.0 3.6 fusion.50
  238.6 66.3 %reduce-scatter.2.cloned.1.call-done = f32[32,2048]{1,0:T(8,128)} async-done(((f32[512,2048]{1,0:T(8,128)}), f32[32,2048]{1,0:T(8,128)}) %reduce-scatter.2.cloned.1.call-update) | async-done | bytes 262160 | tf_op jit(solution)/shard_map/reduce_scatter | solution.py:266
  304.9 1.0 add_convert_fusion
  306.2 57.4 %all_to_all.10 = bf16[16,32,2048]{2,1,0:T(8,128)(2,1)S(1)} all-to-all(bf16[16,32,2048]{2,1,0:T(8,128)(2,1)S(1)} %broadcast_in_dim.15), channel_id=1, replica_groups=mesh['sp_0'=8,'sp_1'=4,'tp'=16] {'tp'}, dimensions={0} | all-to-all | bytes 4194304 | tf_op jit(solution)/shard_map/all_to_all | solution.py:18
  363.6 1.3 copy.50
  (88 shorter events, 5.9 us)
Async XLA Ops:
  6.5 228.4 %copy-start = (bf16[128,2048]{1,0:T(8,128)(2,1)S(1)}, bf16[128,2048]{1,0:T(8,128)(2,1)}, u32[]{:S(2)}) copy-start(bf16[128,2048]{1,0:T(8,128)(2,1)} %param.29) | copy-start | bytes 1572868
  6.5 63.2 %copy-start.1 = (bf16[512,2048]{1,0:T(8,128)(2,1)S(1)}, bf16[512,2048]{1,0:T(8,128)(2,1)}, u32[]{:S(2)}) copy-start(bf16[512,2048]{1,0:T(8,128)(2,1)} %param.15) | copy-start | bytes 6291460
  6.5 63.2 %copy-start.8 = (bf16[2048,128]{1,0:T(8,128)(2,1)S(1)}, bf16[2048,128]{1,0:T(8,128)(2,1)}, u32[]{:S(2)}) copy-start(bf16[2048,128]{1,0:T(8,128)(2,1)} %param.25) | copy-start | bytes 1572868
  11.5 22.8 %all-to-all-start = ((f32[32,3,2,128]{3,2,1,0:T(2,128)}), f32[32,3,2,128]{3,2,1,0:T(2,128)S(1)}, u32[]{:S(2)}, u32[]{:S(2)}) async-start(f32[32,3,2,128]{3,2,1,0:T(2,128)} %broadcast_in_dim.13), calls=%async_computation | async-start | bytes 196608 | tf_op jit(solution)/shard_map/all_to_all | solution.py:18
  25.3 193.9 %all-reduce.6.cloned.1.call-start = ((), (), s32[]{:S(2)}) async-start(), calls=%async_computation.3 | async-start | bytes 262144 | tf_op jit(solution)/shard_map/psum | solution.py:28
  34.4 4.0 %collective-permute-start = (f32[3,2,128]{2,1,0:T(2,128)S(1)}, f32[3,2,128]{2,1,0:T(2,128)S(1)}, u32[]{:S(2)}, u32[]{:S(2)}) collective-permute-start(f32[3,2,128]{2,1,0:T(2,128)S(1)} %reduce_sum.36), channel_id=1, source_target_pairs={{0,1},{1,2},{2,3},{3,4},{4,5},{5,6},{6,7},{7,8},{8,9},{9,10},{10,1... | collective-permute-start | bytes 9224 | tf_op jit(solution)/shard_map/ppermute | solution.py:161
  37.7 3.0 collective-permute-start.1
  38.4 3.0 collective-permute-start.2
  40.7 3.3 collective-permute-start.3
  41.5 4.2 %collective-permute-start.4 = (f32[3,2,128]{2,1,0:T(2,128)S(1)}, f32[3,2,128]{2,1,0:T(2,128)S(1)}, u32[]{:S(2)}, u32[]{:S(2)}) collective-permute-start(f32[3,2,128]{2,1,0:T(2,128)S(1)} %collective-permute-done.2), channel_id=1, source_target_pairs={{0,1},{1,2},{2,3},{3,4},{4,5},{5,6},{6,7},{7,8},{8,9},{9,10},{10,1... | collective-permute-start | bytes 9224 | tf_op jit(solution)/shard_map/ppermute | solution.py:161
  44.0 3.0 collective-permute-start.5
  45.6 4.2 %collective-permute-start.6 = (f32[3,2,128]{2,1,0:T(2,128)S(1)}, f32[3,2,128]{2,1,0:T(2,128)S(1)}, u32[]{:S(2)}, u32[]{:S(2)}) collective-permute-start(f32[3,2,128]{2,1,0:T(2,128)S(1)} %collective-permute-done.4), channel_id=1, source_target_pairs={{0,1},{1,2},{2,3},{3,4},{4,5},{5,6},{6,7},{7,8},{8,9},{9,10},{10,1... | collective-permute-start | bytes 9224 | tf_op jit(solution)/shard_map/ppermute | solution.py:161
  47.1 3.0 collective-permute-start.7
  49.9 4.2 %collective-permute-start.8 = (f32[3,2,128]{2,1,0:T(2,128)S(1)}, f32[3,2,128]{2,1,0:T(2,128)S(1)}, u32[]{:S(2)}, u32[]{:S(2)}) collective-permute-start(f32[3,2,128]{2,1,0:T(2,128)S(1)} %collective-permute-done.6), channel_id=1, source_target_pairs={{0,1},{1,2},{2,3},{3,4},{4,5},{5,6},{6,7},{7,8},{8,9},{9,10},{10,1... | collective-permute-start | bytes 9224 | tf_op jit(solution)/shard_map/ppermute | solution.py:161
  50.1 4.2 %collective-permute-start.9 = (f32[3,2,128]{2,1,0:T(2,128)S(1)}, f32[3,2,128]{2,1,0:T(2,128)S(1)}, u32[]{:S(2)}, u32[]{:S(2)}) collective-permute-start(f32[3,2,128]{2,1,0:T(2,128)S(1)} %collective-permute-done.7), channel_id=1, source_target_pairs={{0,15},{1,0},{2,1},{3,2},{4,3},{5,4},{6,5},{7,6},{8,7},{9,8},{10,9... | collective-permute-start | bytes 9224 | tf_op jit(solution)/shard_map/ppermute | solution.py:164
  54.1 4.2 %collective-permute-start.10 = (f32[3,2,128]{2,1,0:T(2,128)S(1)}, f32[3,2,128]{2,1,0:T(2,128)S(1)}, u32[]{:S(2)}, u32[]{:S(2)}) collective-permute-start(f32[3,2,128]{2,1,0:T(2,128)S(1)} %collective-permute-done.8), channel_id=1, source_target_pairs={{0,1},{1,2},{2,3},{3,4},{4,5},{5,6},{6,7},{7,8},{8,9},{9,10},{10,1... | collective-permute-start | bytes 9224 | tf_op jit(solution)/shard_map/ppermute | solution.py:161
  54.3 4.2 %collective-permute-start.11 = (f32[3,2,128]{2,1,0:T(2,128)S(1)}, f32[3,2,128]{2,1,0:T(2,128)S(1)}, u32[]{:S(2)}, u32[]{:S(2)}) collective-permute-start(f32[3,2,128]{2,1,0:T(2,128)S(1)} %collective-permute-done.9), channel_id=1, source_target_pairs={{0,15},{1,0},{2,1},{3,2},{4,3},{5,4},{6,5},{7,6},{8,7},{9,8},{10,9... | collective-permute-start | bytes 9224 | tf_op jit(solution)/shard_map/ppermute | solution.py:164
  58.3 4.2 %collective-permute-start.12 = (f32[3,2,128]{2,1,0:T(2,128)S(1)}, f32[3,2,128]{2,1,0:T(2,128)S(1)}, u32[]{:S(2)}, u32[]{:S(2)}) collective-permute-start(f32[3,2,128]{2,1,0:T(2,128)S(1)} %collective-permute-done.10), channel_id=1, source_target_pairs={{0,1},{1,2},{2,3},{3,4},{4,5},{5,6},{6,7},{7,8},{8,9},{9,10},{10,1... | collective-permute-start | bytes 9224 | tf_op jit(solution)/shard_map/ppermute | solution.py:161
  58.5 4.2 %collective-permute-start.13 = (f32[3,2,128]{2,1,0:T(2,128)S(1)}, f32[3,2,128]{2,1,0:T(2,128)S(1)}, u32[]{:S(2)}, u32[]{:S(2)}) collective-permute-start(f32[3,2,128]{2,1,0:T(2,128)S(1)} %collective-permute-done.11), channel_id=1, source_target_pairs={{0,15},{1,0},{2,1},{3,2},{4,3},{5,4},{6,5},{7,6},{8,7},{9,8},{10,9... | collective-permute-start | bytes 9224 | tf_op jit(solution)/shard_map/ppermute | solution.py:164
  62.6 4.2 %collective-permute-start.14 = (f32[3,2,128]{2,1,0:T(2,128)S(1)}, f32[3,2,128]{2,1,0:T(2,128)S(1)}, u32[]{:S(2)}, u32[]{:S(2)}) collective-permute-start(f32[3,2,128]{2,1,0:T(2,128)S(1)} %collective-permute-done.12), channel_id=1, source_target_pairs={{0,1},{1,2},{2,3},{3,4},{4,5},{5,6},{6,7},{7,8},{8,9},{9,10},{10,1... | collective-permute-start | bytes 9224 | tf_op jit(solution)/shard_map/ppermute | solution.py:161
  69.7 235.2 %reduce-scatter.2.cloned.1.call-start = ((), (), s32[]{:S(2)}) async-start(), calls=%async_computation.4 | async-start | bytes 4456448 | tf_op jit(solution)/shard_map/reduce_scatter | solution.py:266
  72.7 77.7 %copy-start.4 = (bf16[512,512]{0,1:T(8,128)(2,1)}, bf16[512,512]{0,1:T(8,128)(2,1)S(1)}, u32[]{:S(2)}) copy-start(bf16[512,512]{0,1:T(8,128)(2,1)S(1)} %fusion.18) | copy-start | bytes 1572868
  73.3 77.1 %copy-start.5 = (f32[512,1,32]{0,2,1:T(8,128)}, f32[512,1,32]{0,2,1:T(8,128)S(1)}, u32[]{:S(2)}) copy-start(f32[512,1,32]{0,2,1:T(8,128)S(1)} %get-tuple-element.25) | copy-start | bytes 196612
  73.3 77.1 %copy-start.6 = (f32[512,1,32]{0,2,1:T(8,128)}, f32[512,1,32]{0,2,1:T(8,128)S(1)}, u32[]{:S(2)}) copy-start(f32[512,1,32]{0,2,1:T(8,128)S(1)} %get-tuple-element.26) | copy-start | bytes 196612
  73.3 77.1 %copy-start.7 = (f32[512,1,32]{0,2,1:T(8,128)}, f32[512,1,32]{0,2,1:T(8,128)S(1)}, u32[]{:S(2)}) copy-start(f32[512,1,32]{0,2,1:T(8,128)S(1)} %get-tuple-element.27) | copy-start | bytes 196612
  123.5 25.3 %copy-start.2 = (f32[8,129,128]{2,1,0:T(8,128)}, f32[8,129,128]{2,1,0:T(8,128)S(1)}, u32[]{:S(2)}) copy-start(f32[8,129,128]{2,1,0:T(8,128)S(1)} %all-gather.7) | copy-start | bytes 1585156
  146.8 2.0 copy-start.3
Sparse Core Ops, SparseCore 0:
  69.8 149.2 all-reduce.5
  238.7 66.1 reduce-scatter.1
